TPU v7x, 32 devices: a whole 2x2x4 slice. The times are simulated.
32 devices in a mesh: rep: 2 (over y), fs: 4 (over z), tp: 4 (over x, core).
Axes of the slice: x: 2, y: 2, z: 4, core: 2. Of those that a mesh axis runs over, the one named last changes fastest.
Arguments:
- tokens: bfloat16 [4096, 2048], P(('rep', 'fs'), 'tp'), may hold values from -6 to 6
- outer_gate: float32 [2048, 512], P('fs', 'tp'), may hold values from -0.125 to 0.125
- inner_gate: float32 [2048, 512], P('fs', 'tp'), may hold values from -0.125 to 0.125
- mixer_value: float32 [2048, 512], P('fs', 'tp'), may hold values from -0.125 to 0.125
- mixer_scales: float32 [3, 512], P(None, 'tp'), may hold values from 0.5 to 2
- mixer_taps: float32 [3, 512], P(None, 'tp'), may hold values from -3.5 to 3.5
- mixer_out: float32 [512, 2048], P('fs', 'tp'), may hold values from -0.25 to 0.25
- out_scale: float32 [2048], P('tp'), may hold values from 0.3 to 3
- first_gain: float32 [2048], replicated, may hold values from 0.1 to 1.9
- first_shift: float32 [2048], replicated, may hold values from -2 to 2
- up_proj: float32 [2048, 3072], P('fs', 'tp'), may hold values from -0.125 to 0.125
- gate_proj: float32 [2048, 3072], P('fs', 'tp'), may hold values from -0.125 to 0.125
- up_scales: float32 [2, 3072], P(None, 'tp'), may hold values from 0.5 to 2
- ffn_taps: float32 [3, 2, 3072], P(None, None, 'tp'), may hold values from -3.5 to 3.5
- ffn_shift: float32 [2, 3072], P(None, 'tp'), may hold values from -3 to 3
- down_proj: float32 [3072, 2048], P('fs', 'tp'), may hold values from -0.109375 to 0.109375
- down_scale: float32 [2048], P('tp'), may hold values from 0.3 to 3
- second_gain: float32 [2048], replicated, may hold values from 0.1 to 1.9
- second_shift: float32 [2048], replicated, may hold values from -2 to 2
Outputs:
- layer_out: bfloat16 [4096, 2048], P(('rep', 'fs'), 'tp')
All inputs are finite; a program needn't handle non-finite values.
Results may differ from a plain program's by a relative error of at most 0.017.
Values may be sent and summed in bfloat16 or wider, within the bound.
A program may use at most 64 MiB of HBM per device.

v0:
```python
import jax
import jax.numpy as jnp
from jax import lax
from jax.sharding import PartitionSpec as P

LEN = 128
norm_eps = 1e-05
residual_weight = 8.0**0.25


def causal_mix(signal, kernel_taps):
    sequences = signal.reshape(-1, LEN, signal.shape[-1])
    padded = jnp.pad(sequences, ((0, 0), (2, 0), (0, 0)))
    mixed = (
        kernel_taps[0] * padded[:, :-2]
        + kernel_taps[1] * padded[:, 1:-1]
        + kernel_taps[2] * padded[:, 2:]
    )
    return mixed.reshape(signal.shape)


def lowered(matrix):
    return matrix.astype(jnp.bfloat16)


def single_fold(operand, portion):
    return jnp.dot(operand, portion, preferred_element_type=jnp.float32)


def fold_step(operand, pieces):
    result = []
    for number in range(len(pieces)):
        result.append(jnp.dot(operand, pieces[number], preferred_element_type=jnp.float32))
    return tuple(result)


def own_columns(vector, own_width):
    return lax.dynamic_slice_in_dim(vector, lax.axis_index("tp") * own_width, own_width, 0)


def scaled_norm(summed, average, spread, gain_vector, shift_vector):
    return (summed - average) * lax.rsqrt(spread + norm_eps) * gain_vector + shift_vector


def local(
    tokens,
    outer_gate,
    inner_gate,
    mixer_value,
    mixer_scales,
    mixer_taps,
    mixer_out,
    out_scale,
    first_gain,
    first_shift,
    up_proj,
    gate_proj,
    up_scales,
    ffn_taps,
    ffn_shift,
    down_proj,
    down_scale,
    second_gain,
    second_shift,
):
    own_width = tokens.shape[1]
    full_width = own_width * lax.axis_size("tp")
    token_whole = lax.all_gather(tokens, "tp", axis=1, tiled=True)
    outer_part, inner_part, value_part = fold_step(
        token_whole,
        (
            lax.all_gather(lowered(outer_gate), "fs", axis=0, tiled=True),
            lax.all_gather(lowered(inner_gate), "fs", axis=0, tiled=True),
            lax.all_gather(lowered(mixer_value), "fs", axis=0, tiled=True),
        ),
    )
    outer_part = (outer_part * mixer_scales[0]).astype(jnp.bfloat16)
    inner_part = (inner_part * mixer_scales[1]).astype(jnp.bfloat16)
    value_part = (value_part * mixer_scales[2]).astype(jnp.bfloat16)
    product = inner_part.astype(jnp.float32) * value_part.astype(jnp.float32)
    mixed_conv = (outer_part.astype(jnp.float32) * causal_mix(product, mixer_taps)).astype(
        jnp.bfloat16
    )
    conv_whole = lax.all_gather(mixed_conv, "tp", axis=1, tiled=True)
    mixer_sum = (
        single_fold(conv_whole, lax.all_gather(lowered(mixer_out), "fs", axis=0, tiled=True))
        * out_scale
    )
    first_sum = residual_weight * tokens.astype(jnp.float32) + mixer_sum
    row_total, row_square = lax.psum(
        (jnp.sum(first_sum, 1, keepdims=True), jnp.sum(first_sum * first_sum, 1, keepdims=True)),
        "tp",
    )
    average = row_total / full_width
    spread = row_square / full_width - average * average
    normed = scaled_norm(
        first_sum,
        average,
        spread,
        own_columns(first_gain, own_width),
        own_columns(first_shift, own_width),
    ).astype(jnp.bfloat16)
    normed_whole = lax.all_gather(normed, "tp", axis=1, tiled=True)
    up_matrix, gate_matrix = (
        lax.all_gather(lowered(up_proj), "fs", axis=0, tiled=True),
        lax.all_gather(lowered(gate_proj), "fs", axis=0, tiled=True),
    )
    up_linear = jnp.dot(normed_whole, up_matrix, preferred_element_type=jnp.float32)
    gate_linear = jnp.dot(normed_whole, gate_matrix, preferred_element_type=jnp.float32)
    up_linear = up_linear * up_scales[0]
    gate_linear = gate_linear * up_scales[1]
    up_mixed = causal_mix(up_linear, ffn_taps[:, 0]) + ffn_shift[0]
    gate_mixed = causal_mix(gate_linear, ffn_taps[:, 1]) + ffn_shift[1]
    hidden = (up_mixed * jax.nn.silu(gate_mixed)).astype(jnp.bfloat16)
    hidden_whole = lax.all_gather(hidden, "tp", axis=1, tiled=True)
    ffn_sum = (
        single_fold(hidden_whole, lax.all_gather(lowered(down_proj), "fs", axis=0, tiled=True))
        * down_scale
    )
    second_sum = residual_weight * normed.astype(jnp.float32) + ffn_sum
    second_total, second_square = lax.psum(
        (jnp.sum(second_sum, 1, keepdims=True), jnp.sum(second_sum * second_sum, 1, keepdims=True)),
        "tp",
    )
    second_average = second_total / full_width
    second_spread = second_square / full_width - second_average * second_average
    return scaled_norm(
        second_sum,
        second_average,
        second_spread,
        own_columns(second_gain, own_width),
        own_columns(second_shift, own_width),
    ).astype(jnp.bfloat16)


def solution(mesh):
    return jax.shard_map(
        local,
        mesh=mesh,
        in_specs=(
            P(("rep", "fs"), "tp"),
            P("fs", "tp"),
            P("fs", "tp"),
            P("fs", "tp"),
            P(None, "tp"),
            P(None, "tp"),
            P("fs", "tp"),
            P("tp"),
            P(),
            P(),
            P("fs", "tp"),
            P("fs", "tp"),
            P(None, "tp"),
            P(None, None, "tp"),
            P(None, "tp"),
            P("fs", "tp"),
            P("tp"),
            P(),
            P(),
        ),
        out_specs=P(("rep", "fs"), "tp"),
        check_vma=False,
    )
```

profile of v0, /device:TPU:0, one launch (start us, length us, event | category | flops | bytes accessed | tf_op | source)
XLA Modules:
  0.0 314.0 jit_solution(7180715300881190758)
XLA Ops:
  7.3 2.4 convert_element_type.76
  9.9 1.0 copy.22
  12.5 17.4 %all_gather.36 = bf16[2048,128]{1,0:T(8,128)(2,1)S(1)} all-gather(bf16[512,128]{1,0:T(8,128)(2,1)S(1)} %convert_element_type.69), channel_id=1, replica_groups=mesh['rep'=2,'fs'=4,'tp'=4] {'fs'}, dimensions={0}, use_global_device_ids=true | all-gather | bytes 655360 | tf_op jit(solution)/shard_map/all_gather | solution.py:74
  29.9 16.9 %all_gather.35 = bf16[2048,128]{1,0:T(8,128)(2,1)S(1)} all-gather(bf16[512,128]{1,0:T(8,128)(2,1)S(1)} %convert_element_type.66), channel_id=1, replica_groups=mesh['rep'=2,'fs'=4,'tp'=4] {'fs'}, dimensions={0}, use_global_device_ids=true | all-gather | bytes 655360 | tf_op jit(solution)/shard_map/all_gather | solution.py:73
  46.8 22.6 %all_gather.34 = bf16[2048,128]{1,0:T(8,128)(2,1)S(1)} all-gather(bf16[512,128]{1,0:T(8,128)(2,1)S(1)} %convert_element_type.63), channel_id=1, replica_groups=mesh['rep'=2,'fs'=4,'tp'=4] {'fs'}, dimensions={0}, use_global_device_ids=true | all-gather | bytes 655360 | tf_op jit(solution)/shard_map/all_gather | solution.py:72
  69.4 20.2 %all_gather.38 = bf16[512,512]{1,0:T(8,128)(2,1)S(1)} all-gather(bf16[128,512]{1,0:T(8,128)(2,1)S(1)} %convert_element_type.73), channel_id=1, replica_groups=mesh['rep'=2,'fs'=4,'tp'=4] {'fs'}, dimensions={0}, use_global_device_ids=true | all-gather | bytes 655360 | tf_op jit(solution)/shard_map/all_gather | solution.py:86
  89.6 2.5 fusion.20
  93.7 7.0 %all_gather.37 = bf16[512,512]{1,0:T(8,128)(2,1)S(1)} all-gather(bf16[512,128]{1,0:T(8,128)(2,1)S(1)} %fusion.15), channel_id=1, replica_groups=mesh['rep'=2,'fs'=4,'tp'=4] {'tp'}, dimensions={1}, use_global_device_ids=true | all-gather | bytes 655360 | tf_op jit(solution)/shard_map/all_gather | solution.py:84
  101.3 7.0 %all-reduce.4 = (f32[512,1]{0,1:T(1,128)S(1)}, f32[512,1]{0,1:T(1,128)S(1)}) all-reduce(f32[512,1]{0,1:T(1,128)S(1)} %bitcast.57, f32[512,1]{0,1:T(1,128)S(1)} %bitcast.56), channel_id=1, replica_groups=mesh['rep'=2,'fs'=4,'tp'=4] {'tp'}, use_global_device_ids=true, to_apply=%region_3.4 | all-reduce | flops 1024 | bytes 8192 | tf_op jit(solution)/shard_map/psum | solution.py:90
  108.3 1.0 add_convert_fusion.1
  109.4 1.0 convert_element_type.77
  111.0 1.0 convert_element_type.79
  112.2 2.2 all-gather.11.cloned.1.call-done
  114.4 23.7 %all-gather.9.cloned.1.call-done = bf16[512,2048]{0,1:T(8,128)(2,1)} async-done(((bf16[512,512]{0,1:T(8,128)(2,1)}), bf16[512,2048]{0,1:T(8,128)(2,1)}) %all-gather.9.cloned.1.call-update) | async-done | bytes 2097168 | tf_op jit(solution)/shard_map/all_gather | solution.py:103
  138.2 4.4 %convolution_multiply_fusion.1 = f32[512,768]{1,0:T(8,128)S(1)} fusion(bf16[512,2048]{0,1:T(8,128)(2,1)} %all-gather.9.cloned.1.call-done, bf16[2048,768]{1,0:T(8,128)(2,1)} %all-gather.11.cloned.1.call-done, f32[768]{0:T(1024)S(1)} %get-tuple-element.18), kind=kOutput, calls=%fused_computation.17 | convolution fusion | flops 1611005952 | bytes 6818816 | tf_op jit(solution)/shard_map/dot_general | solution.py:108
  142.5 60.5 %all-gather.13.cloned.1.call-done = bf16[2048,768]{1,0:T(8,128)(2,1)} async-done(((bf16[512,768]{1,0:T(8,128)(2,1)}), bf16[2048,768]{1,0:T(8,128)(2,1)}) %all-gather.13.cloned.1.call-update) | async-done | bytes 3145744 | tf_op jit(solution)/shard_map/all_gather | solution.py:106
  203.1 4.4 %convolution_multiply_fusion = f32[512,768]{1,0:T(8,128)S(1)} fusion(bf16[512,2048]{0,1:T(8,128)(2,1)} %all-gather.9.cloned.1.call-done, bf16[2048,768]{1,0:T(8,128)(2,1)} %all-gather.13.cloned.1.call-done, f32[768]{0:T(1024)S(1)} %get-tuple-element.17), kind=kOutput, calls=%fused_computation.16 | convolution fusion | flops 1611005952 | bytes 6818816 | tf_op jit(solution)/shard_map/dot_general | solution.py:109
  207.4 0.9 fusion.2
  208.4 1.4 fusion.9
  211.3 55.3 %all-gather.17.cloned.1.call-done = bf16[3072,512]{1,0:T(8,128)(2,1)} async-done(((bf16[768,512]{1,0:T(8,128)(2,1)}), bf16[3072,512]{1,0:T(8,128)(2,1)}) %all-gather.17.cloned.1.call-update) | async-done | bytes 3145744 | tf_op jit(solution)/shard_map/all_gather | solution.py:117
  266.6 28.6 %all-gather.15.cloned.1.call-done = bf16[512,3072]{1,0:T(8,128)(2,1)} async-done(((bf16[512,768]{1,0:T(8,128)(2,1)}), bf16[512,3072]{1,0:T(8,128)(2,1)}) %all-gather.15.cloned.1.call-update) | async-done | bytes 3145744 | tf_op jit(solution)/shard_map/all_gather | solution.py:115
  295.2 4.8 %fusion.25 = (f32[512]{0:T(512)S(1)}, f32[512]{0:T(512)S(1)}, f32[512,512]{0,1:T(8,128)S(1)}) fusion(f32[512]{0:T(512)S(1)} %copy-done.16, bf16[512,3072]{1,0:T(8,128)(2,1)} %all-gather.15.cloned.1.call-done, bf16[3072,512]{1,0:T(8,128)(2,1)} %all-gather.17.cloned.1.call-done, bf16[512,512]{0,1:T(8,128)(2,1)S(1)} %copy-done.1), kind=kOutput, calls=%fused_computation.64 | convolution fusion | flops 1612446720 | bytes 7870464 | tf_op jit(solution)/shard_map/dot_general | solution.py:27
  300.0 5.9 %all-reduce.3 = (f32[512,1]{0,1:T(1,128)S(1)}, f32[512,1]{0,1:T(1,128)S(1)}) all-reduce(f32[512,1]{0,1:T(1,128)S(1)} %bitcast.59, f32[512,1]{0,1:T(1,128)S(1)} %bitcast.58), channel_id=1, replica_groups=mesh['rep'=2,'fs'=4,'tp'=4] {'tp'}, use_global_device_ids=true, to_apply=%region_7.8 | all-reduce | flops 1024 | bytes 8192 | tf_op jit(solution)/shard_map/psum | solution.py:121
  306.1 1.0 copy.23
  (67 shorter events, 7.2 us)
Async XLA Ops:
  6.5 83.1 %all-gather.7.cloned.1.call-start = ((), (), s32[]{:S(2)}) async-start(), calls=%async_computation | async-start | bytes 2621440 | tf_op jit(solution)/shard_map/all_gather | solution.py:68
  7.3 2.6 copy-start.2
  7.3 3.6 %copy-start.6 = (f32[512,128]{1,0:T(8,128)S(1)}, f32[512,128]{1,0:T(8,128)}, u32[]{:S(2)}) copy-start(f32[512,128]{1,0:T(8,128)} %param.22) | copy-start | bytes 786436
  7.3 107.2 %all-gather.11.cloned.1.call-start = ((), (), s32[]{:S(2)}) async-start(), calls=%async_computation.2 | async-start | bytes 3932160 | tf_op jit(solution)/shard_map/all_gather | solution.py:105
  9.8 1.1 copy-start.7
  9.8 1.2 copy-start.8
  9.8 1.2 copy-start.9
  9.8 128.4 %all-gather.9.cloned.1.call-start = ((), (), s32[]{:S(2)}) async-start(), calls=%async_computation.1 | async-start | bytes 2621440 | tf_op jit(solution)/shard_map/all_gather | solution.py:103
  11.0 78.6 %copy-start.13 = (f32[3,128]{1,0:T(4,128)S(1)}, f32[3,128]{1,0:T(4,128)}, u32[]{:S(2)}) copy-start(f32[3,128]{1,0:T(4,128)} %param.23) | copy-start | bytes 4612
  11.0 78.6 %copy-start.14 = (f32[3,128]{1,0:T(4,128)S(1)}, f32[3,128]{1,0:T(4,128)}, u32[]{:S(2)}) copy-start(f32[3,128]{1,0:T(4,128)} %param.24) | copy-start | bytes 4612
  89.6 2.5 copy-start
  92.9 7.8 %copy-start.5 = (bf16[512,512]{0,1:T(8,128)(2,1)S(1)}, bf16[512,512]{0,1:T(8,128)(2,1)}, u32[]{:S(2)}) copy-start(bf16[512,512]{0,1:T(8,128)(2,1)} %copy.22) | copy-start | bytes 1572868
  92.9 7.8 %copy-start.15 = (f32[512]{0:T(512)S(1)}, f32[512]{0:T(512)}, u32[]{:S(2)}) copy-start(f32[512]{0:T(512)} %param.26) | copy-start | bytes 6148
  101.3 8.1 %copy-start.3 = (f32[512,768]{1,0:T(8,128)S(1)}, f32[512,768]{1,0:T(8,128)}, u32[]{:S(2)}) copy-start(f32[512,768]{1,0:T(8,128)} %param.30) | copy-start | bytes 4718596
  109.3 1.7 copy-start.4
  109.3 93.8 %all-gather.13.cloned.1.call-start = ((), (), s32[]{:S(2)}) async-start(), calls=%async_computation.3 | async-start | bytes 3932160 | tf_op jit(solution)/shard_map/all_gather | solution.py:106
  110.4 1.6 copy-start.11
  110.4 1.7 copy-start.12
  110.4 1.7 copy-start.10
  110.5 156.2 %all-gather.17.cloned.1.call-start = ((), (), s32[]{:S(2)}) async-start(), calls=%async_computation.5 | async-start | bytes 3932160 | tf_op jit(solution)/shard_map/all_gather | solution.py:117
  112.0 183.2 %all-gather.15.cloned.1.call-start = ((), (), s32[]{:S(2)}) async-start(), calls=%async_computation.4 | async-start | bytes 3932160 | tf_op jit(solution)/shard_map/all_gather | solution.py:115
  208.4 86.8 %copy-start.1 = (bf16[512,512]{0,1:T(8,128)(2,1)S(1)}, bf16[512,512]{0,1:T(8,128)(2,1)}, u32[]{:S(2)}) copy-start(bf16[512,512]{0,1:T(8,128)(2,1)} %add_convert_fusion.1) | copy-start | bytes 1572868
  208.4 86.8 %copy-start.16 = (f32[512]{0:T(512)S(1)}, f32[512]{0:T(512)}, u32[]{:S(2)}) copy-start(f32[512]{0:T(512)} %param.35) | copy-start | bytes 6148
Sparse Core Ops, SparseCore 0:
  8.9 25.2 all-gather.6
  35.8 78.6 all-gather.10
  116.0 22.1 all-gather.8
  139.6 63.4 all-gather.12
  204.5 62.0 all-gather.16
  268.0 27.1 all-gather.14
where the time goes:
time: 314 us
  waiting for transfers between devices  171 us (54%)
  blocking collectives  96.9 us (31%)
  matrix products  18 us (6%)
  between operations  13.8 us (4%)
  other arithmetic  8.13 us (3%)
  local copies, waits for them, and re-layouts  5.76 us (2%)
    all_gather x1, waiting for transfers between devices, local(): lax.all_gather(lowered(gate_proj), 'fs', axis=0, tiled=True)  60.5 us
    all_gather x1, waiting for transfers between devices, local(): lax.all_gather(lowered(down_proj), 'fs', axis=0, tiled=True)  55.3 us
    all_gather x1, waiting for transfers between devices, local(): hidden_whole = lax.all_gather(hidden, 'tp', axis=1, tiled=True)  28.6 us
    all_gather x1, waiting for transfers between devices, local(): normed_whole = lax.all_gather(normed, 'tp', axis=1, tiled=True)  23.7 us
    all_gather x1, blocking collectives, local(): lax.all_gather(lowered(outer_gate), 'fs', axis=0, tiled=True)  22.6 us
    all_gather x1, blocking collectives, local(): lax.all_gather(lowered(mixer_out), 'fs', axis=0, tiled=True)  20.2 us
    all_gather x1, blocking collectives, local(): lax.all_gather(lowered(mixer_value), 'fs', axis=0, tiled=True)  17.4 us
    all_gather x1, blocking collectives, local(): lax.all_gather(lowered(inner_gate), 'fs', axis=0, tiled=True)  16.9 us
  transfers between devices with their start and end apart: 6, of which 5 were waited for; matrix products, arithmetic and copies ran while one was open for 8% of the time, Pallas kernels for 0%

commit v1 on v0

--- a/solution.py
+++ b/solution.py
@@ -1,3 +1,4 @@
+import functools
 import jax
 import jax.numpy as jnp
 from jax import lax
@@ -6,6 +7,23 @@
 LEN = 128
 norm_eps = 1e-05
 residual_weight = 8.0**0.25
+
+
+def _compute_scales(u_in, axis_id):
+    num = lax.axis_size(axis_id)
+    samples = [(i, (i + 1) % num) for i in range(num)]
+    g_now = [None] * num
+    g_now[num - 1] = u_in
+    for d in range(num - 2, -1, -1):
+        g_now[d] = lax.ppermute(g_now[d + 1], axis_id, perm=samples)
+    main = jnp.concatenate(g_now, 1)
+    tile_out = lax.axis_index(axis_id)
+    left_arr = (tile_out + 1) * u_in.shape[1]
+    b_next = jnp.roll(main, left_arr, 1)
+    return b_next
+
+
+_arrange_sheets = functools.partial(_compute_scales, axis_id="tp")
 
 
 def causal_mix(signal, kernel_taps):
@@ -100,7 +118,7 @@
         own_columns(first_gain, own_width),
         own_columns(first_shift, own_width),
     ).astype(jnp.bfloat16)
-    normed_whole = lax.all_gather(normed, "tp", axis=1, tiled=True)
+    normed_whole = _arrange_sheets(normed)
     up_matrix, gate_matrix = (
         lax.all_gather(lowered(up_proj), "fs", axis=0, tiled=True),
         lax.all_gather(lowered(gate_proj), "fs", axis=0, tiled=True),

time: 314 us -> 290 us (0.924)
  waiting for transfers between devices: 171 us -> 142 us
  local copies, waits for them, and re-layouts: 5.76 us -> 9.98 us
    all_gather x1, waiting for transfers between devices: 60.5 us -> 0.01 us  [local(): lax.all_gather(lowered(gate_proj), 'fs', axis=0, tiled=True)]
    all_gather x1, waiting for transfers between devices: 2.23 us -> 31.3 us  [local(): lax.all_gather(lowered(up_proj), 'fs', axis=0, tiled=True)]
    ppermute x0 -> x3, waiting for transfers between devices: none -> 25.7 us  [_compute_scales(): g_now[d] = lax.ppermute(g_now[d + 1], axis_id, perm=samples)]
    all_gather x1 -> x0, waiting for transfers between devices: 23.7 us -> none  [local(): normed_whole = lax.all_gather(normed, 'tp', axis=1, tiled=True)]
    unnamed x35 -> x37, local copies, waits for them, and re-layouts: 1.59 us -> 5.81 us
  transfers between devices with their start and end apart: 6 -> 8, of which waited for: 5 -> 6; matrix products, arithmetic and copies ran while one was open for 8% -> 11% of each run, Pallas kernels for 0% -> 0%
where the time goes in v1:
time: 290 us
  waiting for transfers between devices  142 us (49%)
  blocking collectives  97.2 us (34%)
  matrix products  18 us (6%)
  between operations  13.4 us (5%)
  local copies, waits for them, and re-layouts  9.98 us (3%)
  other arithmetic  9.29 us (3%)
    all_gather x1, waiting for transfers between devices, local(): lax.all_gather(lowered(down_proj), 'fs', axis=0, tiled=True)  55.3 us
    all_gather x1, waiting for transfers between devices, local(): lax.all_gather(lowered(up_proj), 'fs', axis=0, tiled=True)  31.3 us
    all_gather x1, waiting for transfers between devices, local(): hidden_whole = lax.all_gather(hidden, 'tp', axis=1, tiled=True)  28.6 us
    ppermute x3, waiting for transfers between devices, _compute_scales(): g_now[d] = lax.ppermute(g_now[d + 1], axis_id, perm=samples)  25.7 us
    all_gather x1, blocking collectives, local(): lax.all_gather(lowered(outer_gate), 'fs', axis=0, tiled=True)  23.2 us
    all_gather x1, blocking collectives, local(): lax.all_gather(lowered(mixer_out), 'fs', axis=0, tiled=True)  20.1 us
    all_gather x1, blocking collectives, local(): lax.all_gather(lowered(mixer_value), 'fs', axis=0, tiled=True)  17.4 us
    all_gather x1, blocking collectives, local(): lax.all_gather(lowered(inner_gate), 'fs', axis=0, tiled=True)  16.8 us
  transfers between devices with their start and end apart: 8, of which 6 were waited for; matrix products, arithmetic and copies ran while one was open for 11% of the time, Pallas kernels for 0%

profile of v1, /device:TPU:0, one launch (start us, length us, event | category | flops | bytes accessed | tf_op | source)
XLA Modules:
  0.0 289.7 jit_solution(9243595630912566032)
XLA Ops:
  7.3 2.4 convert_element_type.77
  9.8 1.0 convert_element_type.76
  11.4 1.0 convert_element_type.79
  12.7 17.4 %all_gather.33 = bf16[2048,128]{1,0:T(8,128)(2,1)S(1)} all-gather(bf16[512,128]{1,0:T(8,128)(2,1)S(1)} %convert_element_type.69), channel_id=1, replica_groups=mesh['rep'=2,'fs'=4,'tp'=4] {'fs'}, dimensions={0}, use_global_device_ids=true | all-gather | bytes 655360 | tf_op jit(solution)/shard_map/all_gather | solution.py:92
  30.1 16.8 %all_gather.32 = bf16[2048,128]{1,0:T(8,128)(2,1)S(1)} all-gather(bf16[512,128]{1,0:T(8,128)(2,1)S(1)} %convert_element_type.66), channel_id=1, replica_groups=mesh['rep'=2,'fs'=4,'tp'=4] {'fs'}, dimensions={0}, use_global_device_ids=true | all-gather | bytes 655360 | tf_op jit(solution)/shard_map/all_gather | solution.py:91
  47.0 23.2 %all_gather.31 = bf16[2048,128]{1,0:T(8,128)(2,1)S(1)} all-gather(bf16[512,128]{1,0:T(8,128)(2,1)S(1)} %convert_element_type.63), channel_id=1, replica_groups=mesh['rep'=2,'fs'=4,'tp'=4] {'fs'}, dimensions={0}, use_global_device_ids=true | all-gather | bytes 655360 | tf_op jit(solution)/shard_map/all_gather | solution.py:90
  70.3 20.1 %all_gather.35 = bf16[512,512]{1,0:T(8,128)(2,1)S(1)} all-gather(bf16[128,512]{1,0:T(8,128)(2,1)S(1)} %convert_element_type.73), channel_id=1, replica_groups=mesh['rep'=2,'fs'=4,'tp'=4] {'fs'}, dimensions={0}, use_global_device_ids=true | all-gather | bytes 655360 | tf_op jit(solution)/shard_map/all_gather | solution.py:104
  91.9 2.5 fusion.30
  95.9 6.8 %all_gather.34 = bf16[512,512]{1,0:T(8,128)(2,1)S(1)} all-gather(bf16[512,128]{1,0:T(8,128)(2,1)S(1)} %fusion.25), channel_id=1, replica_groups=mesh['rep'=2,'fs'=4,'tp'=4] {'tp'}, dimensions={1}, use_global_device_ids=true | all-gather | bytes 655360 | tf_op jit(solution)/shard_map/all_gather | solution.py:102
  103.3 7.0 %all-reduce.4 = (f32[512,1]{0,1:T(1,128)S(1)}, f32[512,1]{0,1:T(1,128)S(1)}) all-reduce(f32[512,1]{0,1:T(1,128)S(1)} %bitcast.59, f32[512,1]{0,1:T(1,128)S(1)} %bitcast.58), channel_id=1, replica_groups=mesh['rep'=2,'fs'=4,'tp'=4] {'tp'}, use_global_device_ids=true, to_apply=%region_3.4 | all-reduce | flops 1024 | bytes 8192 | tf_op jit(solution)/shard_map/psum | solution.py:108
  110.6 8.6 %collective-permute-done = bf16[512,512]{0,1:T(8,128)(2,1)S(1)} collective-permute-done((bf16[512,512]{0,1:T(8,128)(2,1)S(1)}, bf16[512,512]{0,1:T(8,128)(2,1)S(1)}, u32[]{:S(2)}, u32[]{:S(2)}) %collective-permute-start) | collective-permute-done | bytes 524320 | tf_op jit(solution)/shard_map/ppermute | solution.py:18
  119.2 8.6 %collective-permute-done.1 = bf16[512,512]{0,1:T(8,128)(2,1)S(1)} collective-permute-done((bf16[512,512]{0,1:T(8,128)(2,1)S(1)}, bf16[512,512]{0,1:T(8,128)(2,1)S(1)}, u32[]{:S(2)}, u32[]{:S(2)}) %collective-permute-start.1) | collective-permute-done | bytes 524320 | tf_op jit(solution)/shard_map/ppermute | solution.py:18
  128.0 8.5 %collective-permute-done.2 = bf16[512,512]{0,1:T(8,128)(2,1)S(1)} collective-permute-done((bf16[512,512]{0,1:T(8,128)(2,1)S(1)}, bf16[512,512]{0,1:T(8,128)(2,1)S(1)}, u32[]{:S(2)}, u32[]{:S(2)}) %collective-permute-start.2) | collective-permute-done | bytes 524320 | tf_op jit(solution)/shard_map/ppermute | solution.py:18
  138.9 1.0 constant_dynamic-update-slice_fusion.4
  142.5 1.0 constant_dynamic-update-slice_fusion
  143.5 4.4 %fusion.17 = f32[512,768]{1,0:T(8,128)S(1)} fusion(bf16[2048,768]{1,0:T(8,128)(2,1)} %all-gather.10.cloned.1.call-done, bf16[512,4096]{0,1:T(8,128)(2,1)} %constant_dynamic-update-slice_fusion, s32[]{:T(128)S(6)} %select_n.21, f32[768]{0:T(1024)S(1)} %get-tuple-element.17), kind=kOutput, calls=%fused_computation.21 | convolution fusion | flops 1611005952 | bytes 6818820 | tf_op jit(solution)/shard_map/dot_general | solution.py:127
  147.9 31.3 %all-gather.8.cloned.1.call-done = bf16[2048,768]{1,0:T(8,128)(2,1)} async-done(((bf16[512,768]{1,0:T(8,128)(2,1)}), bf16[2048,768]{1,0:T(8,128)(2,1)}) %all-gather.8.cloned.1.call-update) | async-done | bytes 3145744 | tf_op jit(solution)/shard_map/all_gather | solution.py:123
  179.1 4.4 %fusion.14 = f32[512,768]{1,0:T(8,128)S(1)} fusion(bf16[2048,768]{1,0:T(8,128)(2,1)} %all-gather.8.cloned.1.call-done, bf16[512,4096]{0,1:T(8,128)(2,1)} %constant_dynamic-update-slice_fusion, s32[]{:T(128)S(6)} %select_n.21, f32[768]{0:T(1024)S(1)} %get-tuple-element.18), kind=kOutput, calls=%fused_computation.20 | convolution fusion | flops 1611005952 | bytes 6818820 | tf_op jit(solution)/shard_map/dot_general | solution.py:126
  184.4 1.3 fusion.13
  187.4 55.3 %all-gather.14.cloned.1.call-done = bf16[3072,512]{1,0:T(8,128)(2,1)} async-done(((bf16[768,512]{1,0:T(8,128)(2,1)}), bf16[3072,512]{1,0:T(8,128)(2,1)}) %all-gather.14.cloned.1.call-update) | async-done | bytes 3145744 | tf_op jit(solution)/shard_map/all_gather | solution.py:135
  242.7 28.6 %all-gather.12.cloned.1.call-done = bf16[512,3072]{1,0:T(8,128)(2,1)} async-done(((bf16[512,768]{1,0:T(8,128)(2,1)}), bf16[512,3072]{1,0:T(8,128)(2,1)}) %all-gather.12.cloned.1.call-update) | async-done | bytes 3145744 | tf_op jit(solution)/shard_map/all_gather | solution.py:133
  271.3 4.8 %fusion.37 = (f32[512]{0:T(512)S(1)}, f32[512]{0:T(512)S(1)}, f32[512,512]{0,1:T(8,128)S(1)}) fusion(f32[512]{0:T(512)S(1)} %copy-done.14, bf16[512,3072]{1,0:T(8,128)(2,1)} %all-gather.12.cloned.1.call-done, bf16[3072,512]{1,0:T(8,128)(2,1)} %all-gather.14.cloned.1.call-done, bf16[512,512]{0,1:T(8,128)(2,1)S(1)} %add_convert_fusion.1), kind=kOutput, calls=%fused_computation.78 | convolution fusion | flops 1612446720 | bytes 7870464 | tf_op jit(solution)/shard_map/dot_general | solution.py:45
  276.1 5.9 %all-reduce.3 = (f32[512,1]{0,1:T(1,128)S(1)}, f32[512,1]{0,1:T(1,128)S(1)}) all-reduce(f32[512,1]{0,1:T(1,128)S(1)} %bitcast.61, f32[512,1]{0,1:T(1,128)S(1)} %bitcast.60), channel_id=1, replica_groups=mesh['rep'=2,'fs'=4,'tp'=4] {'tp'}, use_global_device_ids=true, to_apply=%region_7.8 | all-reduce | flops 1024 | bytes 8192 | tf_op jit(solution)/shard_map/psum | solution.py:139
  282.2 1.0 copy.23
  (74 shorter events, 13.5 us)
Async XLA Ops:
  6.5 3.2 %copy-start.2 = (f32[512,768]{1,0:T(8,128)S(1)}, f32[512,768]{1,0:T(8,128)}, u32[]{:S(2)}) copy-start(f32[512,768]{1,0:T(8,128)} %param.29) | copy-start | bytes 4718596
  6.5 85.4 %all-gather.6.cloned.1.call-start = ((), (), s32[]{:S(2)}) async-start(), calls=%async_computation | async-start | bytes 2621440 | tf_op jit(solution)/shard_map/all_gather | solution.py:86
  7.3 136.2 %all-gather.10.cloned.1.call-start = ((), (), s32[]{:S(2)}) async-start(), calls=%async_computation.2 | async-start | bytes 3932160 | tf_op jit(solution)/shard_map/all_gather | solution.py:124
  9.7 1.7 copy-start.3
  9.7 169.4 %all-gather.8.cloned.1.call-start = ((), (), s32[]{:S(2)}) async-start(), calls=%async_computation.1 | async-start | bytes 3932160 | tf_op jit(solution)/shard_map/all_gather | solution.py:123
  10.8 1.7 copy-start.1
  10.8 1.9 copy-start.11
  10.8 1.9 copy-start.4
  10.8 19.3 %copy-start.5 = (f32[512,128]{1,0:T(8,128)S(1)}, f32[512,128]{1,0:T(8,128)}, u32[]{:S(2)}) copy-start(f32[512,128]{1,0:T(8,128)} %param.21) | copy-start | bytes 786436
  10.8 231.9 %all-gather.14.cloned.1.call-start = ((), (), s32[]{:S(2)}) async-start(), calls=%async_computation.4 | async-start | bytes 3932160 | tf_op jit(solution)/shard_map/all_gather | solution.py:135
  12.4 34.6 %copy-start.12 = (f32[3,128]{1,0:T(4,128)S(1)}, f32[3,128]{1,0:T(4,128)}, u32[]{:S(2)}) copy-start(f32[3,128]{1,0:T(4,128)} %param.24) | copy-start | bytes 4612
  12.4 34.6 %copy-start.6 = (f32[512,128]{1,0:T(8,128)S(1)}, f32[512,128]{1,0:T(8,128)}, u32[]{:S(2)}) copy-start(f32[512,128]{1,0:T(8,128)} %param.20) | copy-start | bytes 786436
  12.4 57.9 %copy-start.7 = (f32[128,512]{1,0:T(8,128)S(1)}, f32[128,512]{1,0:T(8,128)}, u32[]{:S(2)}) copy-start(f32[128,512]{1,0:T(8,128)} %param.25) | copy-start | bytes 786436
  12.4 258.9 %all-gather.12.cloned.1.call-start = ((), (), s32[]{:S(2)}) async-start(), calls=%async_computation.3 | async-start | bytes 3932160 | tf_op jit(solution)/shard_map/all_gather | solution.py:133
  91.9 2.5 copy-start
  95.1 7.6 %copy-start.13 = (f32[512]{0:T(512)S(1)}, f32[512]{0:T(512)}, u32[]{:S(2)}) copy-start(f32[512]{0:T(512)} %param.26) | copy-start | bytes 6148
  102.7 25.1 %copy-start.9 = (f32[2,768]{1,0:T(2,128)S(1)}, f32[2,768]{1,0:T(2,128)}, u32[]{:S(2)}) copy-start(f32[2,768]{1,0:T(2,128)} %param.31) | copy-start | bytes 18436
  102.7 25.2 %copy-start.10 = (f32[2,768]{1,0:T(2,128)S(1)}, f32[2,768]{1,0:T(2,128)}, u32[]{:S(2)}) copy-start(f32[2,768]{1,0:T(2,128)} %param.33) | copy-start | bytes 18436
  102.7 25.2 %copy-start.8 = (f32[3,2,768]{2,1,0:T(2,128)S(1)}, f32[3,2,768]{2,1,0:T(2,128)}, u32[]{:S(2)}) copy-start(f32[3,2,768]{2,1,0:T(2,128)} %param.32) | copy-start | bytes 55300
  110.6 8.7 %collective-permute-start = (bf16[512,512]{0,1:T(8,128)(2,1)S(1)}, bf16[512,512]{0,1:T(8,128)(2,1)S(1)}, u32[]{:S(2)}, u32[]{:S(2)}) collective-permute-start(bf16[512,512]{0,1:T(8,128)(2,1)S(1)} %add_convert_fusion.1), channel_id=1, source_target_pairs={{0,1},{1,2},{2,3},{3,0},{4,5},{5,6},{6,7},{7,4},{8,9},{9,10},{10,1... | collective-permute-start | bytes 1572872 | tf_op jit(solution)/shard_map/ppermute | solution.py:18
  119.2 8.6 %collective-permute-start.1 = (bf16[512,512]{0,1:T(8,128)(2,1)S(1)}, bf16[512,512]{0,1:T(8,128)(2,1)S(1)}, u32[]{:S(2)}, u32[]{:S(2)}) collective-permute-start(bf16[512,512]{0,1:T(8,128)(2,1)S(1)} %collective-permute-done), channel_id=1, source_target_pairs={{0,1},{1,2},{2,3},{3,0},{4,5},{5,6},{6,7},{7,4},{8,9},{9,10},{10,1... | collective-permute-start | bytes 1572872 | tf_op jit(solution)/shard_map/ppermute | solution.py:18
  127.8 8.6 %collective-permute-start.2 = (bf16[512,512]{0,1:T(8,128)(2,1)S(1)}, bf16[512,512]{0,1:T(8,128)(2,1)S(1)}, u32[]{:S(2)}, u32[]{:S(2)}) collective-permute-start(bf16[512,512]{0,1:T(8,128)(2,1)S(1)} %collective-permute-done.1), channel_id=1, source_target_pairs={{0,1},{1,2},{2,3},{3,0},{4,5},{5,6},{6,7},{7,4},{8,9},{9,10},{10,1... | collective-permute-start | bytes 1572872 | tf_op jit(solution)/shard_map/ppermute | solution.py:18
  184.4 86.8 %copy-start.14 = (f32[512]{0:T(512)S(1)}, f32[512]{0:T(512)}, u32[]{:S(2)}) copy-start(f32[512]{0:T(512)} %param.35) | copy-start | bytes 6148
Sparse Core Ops, SparseCore 0:
  8.9 25.2 all-gather.5
  35.8 78.5 all-gather.9
  116.0 63.1 all-gather.7
  180.6 62.0 all-gather.13
  244.1 27.1 all-gather.11
